TPU v7x, 32 devices: a whole 2x2x4 slice. The times are simulated.
32 devices in a mesh: gr: 2 (over x), sp: 8 (over z, y), tp: 2 (over core).
Axes of the slice: x: 2, y: 2, z: 4, core: 2. Of those that a mesh axis runs over, the one named last changes fastest.
Arguments:
- prompt: bfloat16 [2, 2048, 4096], P('gr', 'sp', 'tp'), parts along dimension 0, may hold values from -6 to 6
- key_weight: bfloat16 [4096, 4096], P(None, 'tp'), may hold values from -0.09375 to 0.09375
- value_weight: bfloat16 [4096, 4096], P(None, 'tp'), may hold values from -0.375 to 0.375
- beta_weight: bfloat16 [4096, 32], P(None, 'tp'), may hold values from -0.09375 to 0.09375
- beta_bias: float32 [32], P('tp'), may hold values from -4.5 to -0.5
- decay_rate: float32 [32], P('tp'), may hold values from 0.1 to 3
- new_query: bfloat16 [2, 32, 128], P('gr', 'tp'), parts along dimension 0, may hold values from -6 to 6
- read_gain: float32 [128], replicated, may hold values from 0.1 to 1.9
Outputs:
- state_cache: bfloat16 [2, 32, 128, 128], P('gr', 'tp', 'sp'), parts along dimension 0
- first_read: float32 [2, 32, 128], P('gr', 'tp'), parts along dimension 0
There are 2 independent parts, one for each index of `gr`. A program takes and returns all parts, laid end to end along the dimension named above; an argument that names none is the same for every part. Nothing has to cross between parts.
All inputs are finite; a program needn't handle non-finite values.
Results may differ from a plain program's by a relative error of at most 0.013.
Values may be sent and summed in bfloat16 or wider, within the bound.
A program may use at most 128 MiB of HBM per device.

v0:
```python
import jax
import jax.numpy as jnp
from jax import lax
from jax.sharding import PartitionSpec as P

BLOCK = 64


def prefix(value, axis, join, neutral):
    count, mine = (lax.axis_size(axis), lax.axis_index(axis))
    pieces = lax.all_gather(value, axis)
    pieces = pieces[::-1]
    mine = count - 1 - mine
    subtotal = jnp.full_like(value, 0) + jnp.asarray(neutral, value.dtype)

    def lap(position, subtotal):
        longer = join(subtotal, pieces[position])
        return jnp.where(position < mine, longer, subtotal)

    return lax.fori_loop(0, count - 1, lap, subtotal)


def exact_product_sum(pattern, left_side, right_side):
    return jnp.einsum(pattern, left_side, right_side, precision=lax.Precision.HIGHEST)


def block_update(state_carried_over, key_blk, value_blk, beta_blk, log_step):
    span_len = key_blk.shape[1]
    head_dim = key_blk.shape[2]
    steps_in = jnp.arange(1, span_len + 1, dtype=jnp.float32)
    cumulated = log_step[:, None] * steps_in[None, :]
    position = jnp.arange(span_len)
    inclusive = position[:, None] >= position[None, :]
    strictly = position[:, None] > position[None, :]
    log_gap = jnp.where(inclusive, cumulated[:, :, None] - cumulated[:, None, :], 0.0)
    decay_mat = jnp.where(inclusive, jnp.exp(log_gap), 0.0)
    key_gram = exact_product_sum("hcd,hsd->hcs", key_blk, key_blk)
    lower_part = jnp.where(strictly, beta_blk[:, :, None] * key_gram * decay_mat, 0.0)
    system = lower_part + jnp.eye(span_len, dtype=jnp.float32)
    right_hand = jnp.concatenate(
        [value_blk * beta_blk[:, :, None], key_blk * (beta_blk * jnp.exp(cumulated))[:, :, None]],
        axis=-1,
    )
    solved = lax.linalg.triangular_solve(
        system, right_hand, left_side=True, lower=True, unit_diagonal=True
    )
    pseudo_values = solved[:, :, :head_dim]
    surrogate_keys = solved[:, :, head_dim:]
    last_log = cumulated[:, -1]
    key_stop_index = key_blk * jnp.exp(last_log[:, None] - cumulated)[:, :, None]
    written_update = jnp.concatenate([pseudo_values, jnp.zeros_like(pseudo_values)], axis=-1)
    delta_corrected_values = written_update - exact_product_sum(
        "rzt,rtw->rzw", surrogate_keys, state_carried_over
    )
    return jnp.exp(last_log)[:, None, None] * state_carried_over + exact_product_sum(
        "tbq,tbx->tqx", key_stop_index, delta_corrected_values
    )


def shards(
    prompt, key_weight, value_weight, beta_weight, beta_bias, decay_rate, new_query, read_gain
):
    seg_len = prompt.shape[1]
    heads_here = beta_weight.shape[1]
    head_dim = key_weight.shape[1] // heads_here
    full_len = seg_len * lax.axis_size("sp")
    weights = (key_weight, value_weight, beta_weight)
    features = lax.all_gather(prompt, "tp", axis=2, tiled=True)[0]
    key_acc, value_acc, beta_pre = tuple(
        (jnp.dot(features, weight, preferred_element_type=jnp.float32) for weight in weights)
    )
    key_proj = lax.optimization_barrier(key_acc.astype(jnp.bfloat16))
    value_proj = lax.optimization_barrier(value_acc.astype(jnp.bfloat16))
    key_rows = key_proj.astype(jnp.float32).reshape(seg_len, heads_here, head_dim)
    key_rows = key_rows * lax.rsqrt(jnp.sum(key_rows * key_rows, axis=-1, keepdims=True) + 1.0)
    value_rows = value_proj.astype(jnp.float32).reshape(seg_len, heads_here, head_dim)
    strength = jax.nn.sigmoid(beta_pre + beta_bias)
    log_step = -decay_rate / full_len
    key_heads = jnp.transpose(key_rows, (1, 0, 2))
    value_heads = jnp.transpose(value_rows, (1, 0, 2))
    beta_heads = jnp.transpose(strength)
    identity_mat = jnp.broadcast_to(
        jnp.eye(head_dim, dtype=jnp.float32), (heads_here, head_dim, head_dim)
    )
    state_carried_over = jnp.concatenate([jnp.zeros_like(identity_mat), identity_mat], axis=-1)
    for block_start in range(0, seg_len, BLOCK):
        block_end = block_start + BLOCK
        state_carried_over = block_update(
            state_carried_over,
            key_heads[:, block_start:block_end],
            value_heads[:, block_start:block_end],
            beta_heads[:, block_start:block_end],
            log_step,
        )
    own_write = state_carried_over[:, :, :head_dim]
    own_map = state_carried_over[:, :, head_dim:]
    normalized_query = new_query[0].astype(jnp.float32)
    normalized_query = normalized_query * lax.rsqrt(
        jnp.sum(normalized_query * normalized_query, axis=-1, keepdims=True) + 1.0
    )

    def chain_maps(earlier, later):
        return exact_product_sum("hij,hjk->hik", earlier, later)

    later_map = prefix(own_map, "sp", chain_maps, identity_mat)
    own_rows = jnp.transpose(
        lax.psum_scatter(
            exact_product_sum("hkm,hmv->khv", later_map, own_write).astype(jnp.bfloat16),
            "sp",
            scatter_dimension=0,
            tiled=True,
        ).astype(jnp.float32),
        (1, 0, 2),
    )
    pulled = exact_product_sum("hk,hkm->hm", normalized_query, later_map)
    unscaled_read = lax.psum(exact_product_sum("hm,hmv->hv", pulled, own_write), "sp")
    read_out = (
        unscaled_read
        * lax.rsqrt(jnp.mean(unscaled_read * unscaled_read, axis=-1, keepdims=True) + 0.05)
        * read_gain
    )
    return (own_rows.astype(jnp.bfloat16)[None], read_out[None])


def solution(mesh):
    return jax.shard_map(
        shards,
        mesh=mesh,
        in_specs=(
            P("gr", "sp", "tp"),
            P(None, "tp"),
            P(None, "tp"),
            P(None, "tp"),
            P("tp"),
            P("tp"),
            P("gr", "tp", None),
            P(),
        ),
        out_specs=(P("gr", "tp", "sp", None), P("gr", "tp", None)),
        check_vma=False,
    )
```

profile of v0, /device:TPU:0, one launch (start us, length us, event | category | flops | bytes accessed | tf_op | source)
XLA Modules:
  0.0 634.0 jit_solution(10251037068313097658)
XLA Ops:
  9.0 13.8 %all-gather.4.cloned.1.call-done = bf16[1,256,4096]{2,1,0:T(8,128)(2,1)} async-done(((bf16[1,256,2048]{2,1,0:T(8,128)(2,1)}), bf16[1,256,4096]{2,1,0:T(8,128)(2,1)}) %all-gather.4.cloned.1.call-update) | async-done | bytes 2097168 | tf_op jit(solution)/shard_map/all_gather | solution.py:68
  25.4 8.3 %convolution_convert_fusion.1 = bf16[256,2048]{1,0:T(8,128)(2,1)S(1)} fusion(bf16[4096,2048]{1,0:T(8,128)(2,1)} %param.13, bf16[1,256,4096]{2,1,0:T(8,128)(2,1)S(1)} %copy-done.4), kind=kOutput, calls=%fused_computation.11 | convolution fusion | flops 4295491584 | bytes 19922944 | tf_op jit(solution)/shard_map/dot_general | solution.py:70
  36.3 8.3 %convolution_convert_fusion = bf16[256,2048]{1,0:T(8,128)(2,1)S(1)} fusion(bf16[4096,2048]{1,0:T(8,128)(2,1)} %param.14, bf16[1,256,4096]{2,1,0:T(8,128)(2,1)S(1)} %copy-done.4), kind=kOutput, calls=%fused_computation.10 | convolution fusion | flops 4295491584 | bytes 19922944 | tf_op jit(solution)/shard_map/dot_general | solution.py:70
  50.0 78.6 %custom-call.9 = f32[16,1,64,64]{2,3,1,0:T(8,128)S(1)} custom-call(f32[16,1,64,64]{3,2,1,0:T(8,128)S(1)} %fusion.44), custom_call_target="InvertDiagBlocksLowerTriangular" | custom-call | tf_op jit(solution)/shard_map/triangular_solve/custom-call.1 | solution.py:44
  130.5 79.4 %custom-call.8 = f32[16,1,64,64]{2,3,1,0:T(8,128)S(1)} custom-call(f32[16,1,64,64]{3,2,1,0:T(8,128)} %fusion.40), custom_call_target="InvertDiagBlocksLowerTriangular" | custom-call | tf_op jit(solution)/shard_map/triangular_solve/custom-call.1 | solution.py:44
  211.7 80.0 %custom-call.7 = f32[16,1,64,64]{2,3,1,0:T(8,128)} custom-call(f32[16,1,64,64]{3,2,1,0:T(8,128)} %fusion.36), custom_call_target="InvertDiagBlocksLowerTriangular" | custom-call | tf_op jit(solution)/shard_map/triangular_solve/custom-call.1 | solution.py:44
  293.5 80.0 %custom-call.6 = f32[16,1,64,64]{2,3,1,0:T(8,128)} custom-call(f32[16,1,64,64]{3,2,1,0:T(8,128)} %fusion.32), custom_call_target="InvertDiagBlocksLowerTriangular" | custom-call | tf_op jit(solution)/shard_map/triangular_solve/custom-call.1 | solution.py:44
  373.5 2.7 slice_multiply_fusion
  383.4 2.6 multiply_add_fusion.2
  388.4 2.7 multiply_add_fusion.1
  393.6 2.5 multiply_add_fusion
  399.0 125.4 %all-gather.6.cloned.1.call-done = f32[128,128,128]{2,1,0:T(8,128)} async-done(((f32[16,128,128]{2,1,0:T(8,128)}), f32[128,128,128]{2,1,0:T(8,128)}) %all-gather.6.cloned.1.call-update) | async-done | bytes 8388624 | tf_op jit(solution)/shard_map/all_gather | solution.py:11
  524.4 9.4 %copy.70 = f32[8,16,128,128]{2,3,1,0:T(8,128)} copy(f32[8,16,128,128]{3,2,1,0:T(8,128)} %bitcast.106) | data formatting | bytes 16777216 | tf_op jit(solution)/shard_map/all_gather | solution.py:11
  533.8 7.7 %rev.3 = f32[8,16,128,128]{2,3,1,0:T(8,128)} reverse(f32[8,16,128,128]{2,3,1,0:T(8,128)} %copy.70), dimensions={0} | reverse | bytes 16777216 | tf_op jit(solution)/shard_map/rev | solution.py:12
  541.6 18.0 %while.13 = (s32[]{:T(128)}, f32[16,128,128]{1,2,0:T(8,128)S(1)}, s32[]{:T(128)}, f32[8,16,128,128]{2,3,1,0:T(8,128)}, s32[]{:T(128)}) while((s32[]{:T(128)}, f32[16,128,128]{1,2,0:T(8,128)S(1)}, s32[]{:T(128)}, f32[8,16,128,128]{2,3,1,0:T(8,128)}, s32[]{:T(128)}) %tuple.62), condition=%wide.region_2.4_spmd, body=%wide.region_1.0_spmd.sunk | while | flops 402915328 | bytes 6292039 | solution.py:20
  541.7 2.6 fusion.138
  544.4 2.4 fusion.138
  546.9 2.4 fusion.138
  549.5 2.4 fusion.138
  554.6 2.4 fusion.138
  557.2 2.4 fusion.138
  559.6 2.6 fusion.20
  567.3 19.0 %psum.7 = f32[16,128]{1,0:T(8,128)S(1)} all-reduce(f32[16,128]{1,0:T(8,128)S(1)} %bitcast.112), channel_id=1, replica_groups=mesh['gr'=2,'sp'=8,'tp'=2] {'sp'}, use_global_device_ids=true, to_apply=%region_5.7 | all-reduce | flops 2048 | bytes 16384 | tf_op jit(solution)/shard_map/psum | solution.py:116
  587.0 38.5 %reduce-scatter.2.cloned.1.call-done = bf16[16,16,128]{2,1,0:T(8,128)(2,1)} async-done(((bf16[128,16,128]{2,1,0:T(8,128)(2,1)}), bf16[16,16,128]{2,1,0:T(8,128)(2,1)}) %reduce-scatter.2.cloned.1.call-update) | async-done | bytes 65552 | tf_op jit(solution)/shard_map/reduce_scatter | solution.py:107
  (81 shorter events, 42.8 us)
Async XLA Ops:
  7.2 15.7 %copy-start = (bf16[4096,16]{0,1:T(8,128)(2,1)S(1)}, bf16[4096,16]{0,1:T(8,128)(2,1)}, u32[]{:S(2)}) copy-start(bf16[4096,16]{0,1:T(8,128)(2,1)} %param.15) | copy-start | bytes 393220
  7.2 15.7 %all-gather.4.cloned.1.call-start = ((), (), s32[]{:S(2)}) async-start(), calls=%async_computation.1 | async-start | bytes 3145728 | tf_op jit(solution)/shard_map/all_gather | solution.py:68
  7.9 516.5 %all-gather.6.cloned.1.call-start = ((), (), s32[]{:S(2)}) async-start(), calls=%async_computation.3 | async-start | bytes 9437184 | tf_op jit(solution)/shard_map/all_gather | solution.py:11
  22.9 2.5 copy-start.4
  373.5 2.7 copy-start.6
  376.2 1.2 copy-start.8
  378.6 2.1 copy-start.5
  396.1 1.3 copy-start.2
  397.5 1.3 copy-start.7
  398.6 226.9 %reduce-scatter.2.cloned.1.call-start = ((), (), s32[]{:S(2)}) async-start(), calls=%async_computation.2 | async-start | bytes 589824 | tf_op jit(solution)/shard_map/reduce_scatter | solution.py:107
  541.6 18.0 %copy-start.3 = (f32[16,128,256]{2,1,0:T(8,128)S(1)}, f32[16,128,256]{2,1,0:T(8,128)}, u32[]{:S(2)}) copy-start(f32[16,128,256]{2,1,0:T(8,128)} %copy-done.2) | copy-start | bytes 6291460
  559.6 67.4 %copy-start.1 = (bf16[4096,16]{0,1:T(8,128)(2,1)S(1)}, bf16[4096,16]{0,1:T(8,128)(2,1)}, u32[]{:S(2)}) copy-start(bf16[4096,16]{0,1:T(8,128)(2,1)} %param.15) | copy-start | bytes 393220
  562.3 24.1 %copy-start.9 = (f32[128]{0:T(128)S(1)}, f32[128]{0:T(128)}, u32[]{:S(2)}) copy-start(f32[128]{0:T(128)} %param.19) | copy-start | bytes 1540
Sparse Core Ops, SparseCore 0:
  9.5 13.2 all-gather.3
  398.7 125.6 all-gather.5
  564.7 60.8 reduce-scatter.1
where the time goes:
time: 644 us; the launch traced here: 634 us
  other arithmetic  327 us (51%)
  waiting for transfers between devices  178 us (28%)
  matrix products  67.7 us (11%)
  local copies, waits for them, and re-layouts  27.1 us (4%)
  blocking collectives  19 us (3%)
  between operations  14.6 us (2%)
    another operation x7, other arithmetic, block_update(): lax.linalg.triangular_solve(system, right_hand, left_side=True, lower=Tru...  318 us
    all_gather x1, waiting for transfers between devices, prefix(): pieces = lax.all_gather(value, axis)  125 us
    dot_general x22, matrix products, exact_product_sum(): jnp.einsum(pattern, left_side, right_side, precision=lax.Precision.HIGHEST)  44.4 us
    reduce_scatter x1, waiting for transfers between devices, shards(): lax.psum_scatter(exact_product_sum('hkm,hmv->khv', later_map, own_write)....  38.5 us
    psum x1, blocking collectives, shards(): lax.psum(exact_product_sum('hm,hmv->hv', pulled, own_write), 'sp')  19 us
    dot_general x3, matrix products, shards(): jnp.dot(features, weight, preferred_element_type=jnp.float32)  18.9 us
    all_gather x1, waiting for transfers between devices, shards(): features = lax.all_gather(prompt, 'tp', axis=2, tiled=True)[0]  13.8 us
  transfers between devices with their start and end apart: 3, of which 3 were waited for; matrix products, arithmetic and copies ran while one was open for 1% of the time, Pallas kernels for 0%

commit v1 on v0

v1 whole, which is shorter than its diff:
```python
import functools

import jax
import jax.numpy as jnp
from jax import lax
from jax.experimental import pallas as pl
from jax.experimental.pallas import tpu as pltpu
from jax.sharding import PartitionSpec as P

MESH = pl.DeviceIdType.MESH
F32 = jnp.float32
BF16 = jnp.bfloat16


def dot(left, right, contract=((1,), (0,))):
    return lax.dot_general(left, right, (contract, ((), ())), preferred_element_type=F32)


def level_masks(size):
    row = lax.broadcasted_iota(jnp.int32, (size, size), 0)
    col = lax.broadcasted_iota(jnp.int32, (size, size), 1)
    masks = []
    for level in range((size - 1).bit_length()):
        together = (row >> (level + 1)) == (col >> (level + 1))
        apart = (row >> level) != (col >> level)
        masks.append((together & apart & (row > col)).astype(F32).astype(BF16))
    return masks


def span(heads, masks, eye):
    keys_t, rights, grams, inverses = [], [], [], []
    for key, value, strength, fade in heads:
        key = key.astype(F32)
        key = key * lax.rsqrt(jnp.sum(key * key, axis=1, keepdims=True) + 1.0)
        weighted = (key * strength).astype(BF16)
        key = key.astype(BF16)
        value = (value.astype(F32) * (strength * fade)).astype(BF16)
        keys_t.append(key)
        rights.append(jnp.concatenate([value, weighted], axis=1))
        grams.append(dot(weighted, key, ((1,), (1,))).astype(BF16))
    for gram in grams:
        inverses.append(eye[...] - gram * masks[0])
    size = grams[0].shape[0]
    levels = (size - 1).bit_length()
    for level in range(1, levels - 1):
        steps = [dot(g * masks[level], x).astype(BF16) for g, x in zip(grams, inverses)]
        inverses = [x - dot(x, s).astype(BF16) for x, s in zip(inverses, steps)]
    half = size // 2
    out = []
    for key, right, gram, x in zip(keys_t, rights, grams, inverses):
        first, last = x[:half, :half], x[half:, half:]
        cross = dot(last, dot(gram[half:, :half], first).astype(BF16)).astype(BF16)
        top, low = key[:half], key[half:]
        y_first = dot(top, first, ((0,), (0,))) - dot(low, cross, ((0,), (0,)))
        y_last = dot(low, last, ((0,), (0,)))
        y = jnp.concatenate([y_first.astype(BF16), y_last.astype(BF16)], axis=1)
        out.append(dot(y, right))
    return out


def kernel(
    n, tp, groups, per, dim,
    prompt, key_w, value_w, beta_w, bias, decay, query, gain,
    state_out, read_out,
    feat, wbuf, mask_buf, eye_buf, strength_buf, send, recv, row_stage, row_recv, read_stage, read_recv,
    feat_send, feat_recv, w_sem, map_send, map_recv, row_send, row_got, read_send, read_got,
):
    me = lax.axis_index("sp")
    core = lax.axis_index("tp")
    seg, part = prompt.shape[1], prompt.shape[2]

    wide = per * dim
    full = seg * n
    stride = n // groups
    everyone = groups == n
    mine = me // stride
    is_owner = lax.rem(me, stride) == 0

    def when_owner(work):
        if everyone:
            work()
        else:
            pl.when(is_owner)(work)

    def group_at(i):
        return lax.rem(mine + 1 + i, groups)

    def fetch(i):
        at = pl.ds(pl.multiple_of(group_at(i) * wide, wide), wide)
        slot = lax.rem(i, 2)
        return [
            pltpu.make_async_copy(w.at[:, at], wbuf.at[slot, j], w_sem.at[slot, j])
            for j, w in enumerate((key_w, value_w))
        ]

    for copy in fetch(0):
        copy.start()

    barrier = pltpu.get_barrier_semaphore()
    for d in range(1, n):
        pl.semaphore_signal(barrier, inc=1, device_id={"sp": lax.rem(me + d, n)}, device_id_type=MESH)
    for d in range(1, tp):
        pl.semaphore_signal(barrier, inc=1, device_id={"tp": lax.rem(core + d, tp)}, device_id_type=MESH)
    pl.semaphore_wait(barrier, n - 1 + tp - 1)

    def feature_copy(d, slot):
        return pltpu.make_async_remote_copy(
            src_ref=prompt.at[0], dst_ref=feat.at[slot],
            send_sem=feat_send.at[d - 1], recv_sem=feat_recv.at[slot],
            device_id={"tp": lax.rem(core + d, tp)}, device_id_type=MESH,
        )

    for d in range(1, tp):
        feature_copy(d, core).start()

    for level, mask in enumerate(level_masks(seg)):
        mask_buf[level] = mask
    ids = [lax.broadcasted_iota(jnp.int32, (seg, seg), axis) for axis in (0, 1)]
    eye_buf[...] = (ids[0] == ids[1]).astype(F32).astype(BF16)

    def project(weights):
        total = dot(prompt[0], weights[pl.ds(pl.multiple_of(core * part, part), part), :])
        for d in range(1, tp):
            other = lax.rem(core + d, tp)
            total += dot(feat[other], weights[pl.ds(pl.multiple_of(other * part, part), part), :])
        return total

    for d in range(1, tp):
        feature_copy(d, lax.rem(core + d, tp)).wait_recv()
    strength_buf[...] = jax.nn.sigmoid(project(beta_w) + bias[...])

    def map_copy(g):
        return pltpu.make_async_remote_copy(
            src_ref=send.at[g], dst_ref=recv.at[me],
            send_sem=map_send.at[g], recv_sem=map_recv.at[me],
            device_id={"sp": g * stride}, device_id_type=MESH,
        )

    def body(i, carry):
        g = group_at(i)
        slot = lax.rem(i, 2)
        for copy in fetch(i):
            copy.wait()

        @pl.when(i + 1 < groups)
        def _():
            for copy in fetch(i + 1):
                copy.start()

        keys = project(wbuf.at[slot, 0]).astype(BF16)
        values = project(wbuf.at[slot, 1]).astype(BF16)

        @pl.when(i > 0)
        def _():
            map_copy(group_at(i - 1)).start()

        strengths = strength_buf[...]
        lane = lax.broadcasted_iota(jnp.int32, strengths.shape, 1)
        rest = full - 1 - me * seg - lax.broadcasted_iota(jnp.int32, (seg, 1), 0)
        rest = rest.astype(F32) * (1.0 / full)
        heads = []
        for h in range(per):
            head = g * per + h
            strength = jnp.sum(jnp.where(lane == head, strengths, 0.0), axis=1, keepdims=True)
            fade = jnp.exp(-decay[head] * rest)
            cols = slice(h * dim, (h + 1) * dim)
            heads.append((keys[:, cols], values[:, cols], strength, fade))
        for h, result in enumerate(span(heads, mask_buf, eye_buf)):
            send[g, h] = result.astype(BF16)
        return carry

    lax.fori_loop(0, groups, body, 0)

    if not everyone:
        @pl.when(jnp.logical_not(is_owner))
        def _():
            map_copy(mine).start()

    rows = dim // n

    def row_copy(q, slot):
        return pltpu.make_async_remote_copy(
            src_ref=row_stage.at[q], dst_ref=row_recv.at[slot],
            send_sem=row_send.at[q], recv_sem=row_got.at[slot],
            device_id={"sp": q}, device_id_type=MESH,
        )

    def read_copy(q, slot):
        return pltpu.make_async_remote_copy(
            src_ref=read_stage, dst_ref=read_recv.at[slot],
            send_sem=read_send.at[q], recv_sem=read_got.at[slot],
            device_id={"sp": q}, device_id_type=MESH,
        )

    def map_arrival(src):
        return pltpu.make_async_remote_copy(
            src_ref=send.at[0], dst_ref=recv.at[src],
            send_sem=map_send.at[0], recv_sem=map_recv.at[src],
            device_id={"sp": me}, device_id_type=MESH,
        )

    def finish():
        recv[me] = send[mine]

        def link(p, states):
            @pl.when(p != me)
            def _():
                map_arrival(p).wait_recv()

            new = []
            for h in range(per):
                write, drop = recv[p, h, :, :dim].astype(F32), recv[p, h, :, dim:]
                high = states[h].astype(BF16)
                low = (states[h] - high.astype(F32)).astype(BF16)
                new.append(states[h] + (write - dot(drop, high) - dot(drop, low)))
            return tuple(new)

        states = lax.fori_loop(0, n, link, tuple(jnp.zeros((dim, dim), F32) for _ in range(per)))
        for h in range(per):
            cast = states[h].astype(BF16)
            for q in range(n):
                row_stage[q, h] = cast[q * rows:(q + 1) * rows]
        unit = query[0].astype(F32)
        unit = unit * lax.rsqrt(jnp.sum(unit * unit, axis=1, keepdims=True) + 1.0)
        which = lax.broadcasted_iota(jnp.int32, unit.shape, 0)
        for h in range(per):
            row = jnp.sum(jnp.where(which == mine * per + h, unit, 0.0), axis=0, keepdims=True)
            raw = jnp.dot(
                jnp.broadcast_to(row, (8, dim)), states[h],
                precision=lax.Precision.HIGHEST, preferred_element_type=F32,
            )[0:1]
            raw = raw * lax.rsqrt(jnp.mean(raw * raw, axis=1, keepdims=True) + 0.05) * gain[...]
            read_stage[h:h + 1] = raw
        for d in range(1, n):
            row_copy(lax.rem(me + d, n), mine).start()
        for d in range(1, n):
            read_copy(lax.rem(me + d, n), mine).start()
        row_recv[mine] = row_stage[me]
        read_recv[mine] = read_stage[...]

    when_owner(finish)

    for g in range(groups):
        @pl.when(me != g * stride)
        def _():
            row_copy(me, g).wait_recv()
            read_copy(me, g).wait_recv()

        for h in range(per):
            state_out[0, g * per + h] = row_recv[g, h]
        read_out[0, g * per:(g + 1) * per] = read_recv[g]

    for d in range(1, tp):
        feature_copy(d, core).wait_send()
    for g in range(groups):
        @pl.when(me != g * stride)
        def _():
            map_copy(g).wait_send()

    def sent():
        for d in range(1, n):
            row_copy(lax.rem(me + d, n), mine).wait_send()
            read_copy(lax.rem(me + d, n), mine).wait_send()

    when_owner(sent)


def solution(mesh):
    n, tp = mesh.shape["sp"], mesh.shape["tp"]

    def shards(prompt, key_w, value_w, beta_w, bias, decay, query, gain):
        seg, part = prompt.shape[1:]
        depth = key_w.shape[0]
        heads = beta_w.shape[1]
        dim = key_w.shape[1] // heads
        per = max(1, heads // n)
        groups = heads // per
        wide = per * dim
        rows = dim // n
        levels = (seg - 1).bit_length()
        dma = pltpu.SemaphoreType.DMA
        vmem = pl.BlockSpec(memory_space=pltpu.VMEM)
        hbm = pl.BlockSpec(memory_space=pl.ANY)
        return pl.pallas_call(
            functools.partial(kernel, n, tp, groups, per, dim),
            out_shape=(
                jax.ShapeDtypeStruct((1, heads, rows, dim), BF16),
                jax.ShapeDtypeStruct((1, heads, dim), F32),
            ),
            in_specs=[vmem, hbm, hbm, vmem, vmem, pl.BlockSpec(memory_space=pltpu.SMEM), vmem, vmem],
            out_specs=(vmem, vmem),
            scratch_shapes=[
                pltpu.VMEM((tp, seg, part), BF16),
                pltpu.VMEM((2, 2, depth, wide), BF16),
                pltpu.VMEM((levels, seg, seg), BF16),
                pltpu.VMEM((seg, seg), BF16),
                pltpu.VMEM((seg, heads), F32),
                pltpu.VMEM((groups, per, dim, 2 * dim), BF16),
                pltpu.VMEM((n, per, dim, 2 * dim), BF16),
                pltpu.VMEM((n, per, rows, dim), BF16),
                pltpu.VMEM((groups, per, rows, dim), BF16),
                pltpu.VMEM((per, dim), F32),
                pltpu.VMEM((groups, per, dim), F32),
                dma((tp - 1,)),
                dma((tp,)),
                dma((2, 2)),
                dma((groups,)),
                dma((n,)),
                dma((n,)),
                dma((groups,)),
                dma((n,)),
                dma((groups,)),
            ],
            compiler_params=pltpu.CompilerParams(
                collective_id=0, has_side_effects=True, vmem_limit_bytes=48 * 2**20
            ),
        )(prompt, key_w, value_w, beta_w, bias.reshape(1, heads), decay, query, gain.reshape(1, dim))

    return jax.shard_map(
        shards,
        mesh=mesh,
        in_specs=(
            P("gr", "sp", "tp"),
            P(None, "tp"),
            P(None, "tp"),
            P(None, "tp"),
            P("tp"),
            P("tp"),
            P("gr", "tp", None),
            P(),
        ),
        out_specs=(P("gr", "tp", "sp", None), P("gr", "tp", None)),
        check_vma=False,
    )
```

time: 644 us -> 61.6 us (0.10); the launches traced: 634 us -> 61.4 us
  other arithmetic: 327 us -> 0 us
  waiting for transfers between devices: 178 us -> 0 us
  matrix products: 67.7 us -> 0 us
  Pallas kernels: 0 us -> 54.3 us
  local copies, waits for them, and re-layouts: 27.1 us -> 6.48 us
  blocking collectives: 19 us -> 0 us
  between operations: 14.6 us -> 0.66 us
    another operation x7 -> x0, other arithmetic: 318 us -> none  [block_update(): lax.linalg.triangular_solve(system, right_hand, left_side=True, lower=Tru...]
    all_gather x2 -> x0, waiting for transfers between devices: 139 us -> none  [the longest x1 125 us: prefix(): pieces = lax.all_gather(value, axis)]
    dot_general x25 -> x0, matrix products: 63.4 us -> none  [the longest x22 44.4 us: exact_product_sum(): jnp.einsum(pattern, left_side, right_side, precision=lax.Precision.HIGHEST)]
    pallas_call x0 -> x1, Pallas kernels: none -> 54.3 us  [shards(): pl.pallas_call(functools.partial(kernel, n, tp, groups, per, dim), out_sh...]
    reduce_scatter x1 -> x0, waiting for transfers between devices: 38.5 us -> none  [shards(): lax.psum_scatter(exact_product_sum('hkm,hmv->khv', later_map, own_write)....]
    psum x1 -> x0, blocking collectives: 19 us -> none  [shards(): lax.psum(exact_product_sum('hm,hmv->hv', pulled, own_write), 'sp')]
    all_gather x1 -> x0, local copies, waits for them, and re-layouts: 9.38 us -> none  [prefix(): pieces = lax.all_gather(value, axis)]
    rev x1 -> x0, local copies, waits for them, and re-layouts: 7.73 us -> none  [prefix(): pieces = pieces[::-1]]
  transfers between devices with their start and end apart: 3 -> 0, of which waited for: 3 -> 0; matrix products, arithmetic and copies ran while one was open for 1% -> 0% of each run, Pallas kernels for 0% -> 0%
where the time goes in v1:
time: 61.6 us; the launch traced here: 61.4 us
  Pallas kernels  54.3 us (88%)
  local copies, waits for them, and re-layouts  6.48 us (11%)
  between operations  0.66 us (1%)
    pallas_call x1, Pallas kernels, shards(): pl.pallas_call(functools.partial(kernel, n, tp, groups, per, dim), out_sh...  54.3 us
    unnamed x13, local copies, waits for them, and re-layouts  6.48 us

profile of v1, /device:TPU:0, one launch (start us, length us, event | category | flops | bytes accessed | tf_op | source)
XLA Modules:
  0.0 61.4 jit_solution(12734099068897448122)
XLA Ops:
  0.6 1.4 %copy.10.beta_w = bf16[4096,16]{1,0:T(8,128)(2,1)S(1)} copy(bf16[4096,16]{0,1:T(8,128)(2,1)} %param.11) | data formatting | bytes 262144 | tf_op args[3]
  2.0 0.0 copy-start
  2.0 1.2 %copy-done = bf16[1,256,2048]{2,1,0:T(8,128)(2,1)S(1)} copy-done((bf16[1,256,2048]{2,1,0:T(8,128)(2,1)S(1)}, bf16[1,256,2048]{2,1,0:T(8,128)(2,1)}, u32[]{:S(2)}) %copy-start) | copy-done | bytes 1048600
  3.2 0.0 copy-start.1
  3.2 0.7 %copy-done.1 = bf16[1,16,128]{2,1,0:T(8,128)(2,1)S(1)} copy-done((bf16[1,16,128]{2,1,0:T(8,128)(2,1)S(1)}, bf16[1,16,128]{2,1,0:T(8,128)(2,1)}, u32[]{:S(2)}) %copy-start.1) | copy-done | bytes 4120
  3.9 0.0 copy-start.2
  3.9 0.7 %copy-done.2 = f32[16]{0:T(128)S(1)} copy-done((f32[16]{0:T(128)S(1)}, f32[16]{0:T(128)}, u32[]{:S(2)}) %copy-start.2) | copy-done | bytes 88
  4.6 0.0 copy-start.3
  4.6 0.7 %copy-done.3 = f32[16]{0:T(128)S(1)} copy-done((f32[16]{0:T(128)S(1)}, f32[16]{0:T(128)}, u32[]{:S(2)}) %copy-start.3) | copy-done | bytes 88
  5.2 0.0 copy-start.4
  5.2 0.7 %copy-done.4 = f32[128]{0:T(128)S(1)} copy-done((f32[128]{0:T(128)S(1)}, f32[128]{0:T(128)}, u32[]{:S(2)}) %copy-start.4) | copy-done | bytes 536
  5.9 54.3 %shard_map.95 = (bf16[1,16,16,128]{3,2,1,0:T(8,128)(2,1)S(1)}, f32[1,16,128]{2,1,0:T(8,128)S(1)}) custom-call(bf16[1,256,2048]{2,1,0:T(8,128)(2,1)S(1)} %copy-done, bf16[4096,2048]{1,0:T(8,128)(2,1)} %key_w.1, bf16[4096,2048]{1,0:T(8,128)(2,1)} %value_w.1, bf16[4096,16]{1,0:T(8,128)(2,1)S(1)} %copy.10.beta_w, f32[1,16]{1,0:T(1,128)S(1)} %bitcast.2, ...), custom_call_target="tpu_custom_call" | custom-call | tf_op jit(solution)/shard_map/pallas_call | solution.py:284
  60.2 0.6 %copy.13 = bf16[1,16,16,128]{3,2,1,0:T(8,128)(2,1)} copy(bf16[1,16,16,128]{3,2,1,0:T(8,128)(2,1)S(1)} %get-tuple-element.4) | data formatting | bytes 131072
  60.8 0.6 copy.14
Async XLA Ops:
  2.0 1.2 %copy-start = (bf16[1,256,2048]{2,1,0:T(8,128)(2,1)S(1)}, bf16[1,256,2048]{2,1,0:T(8,128)(2,1)}, u32[]{:S(2)}) copy-start(bf16[1,256,2048]{2,1,0:T(8,128)(2,1)} %prompt.1) | copy-start | bytes 3145732
  3.2 0.7 %copy-start.1 = (bf16[1,16,128]{2,1,0:T(8,128)(2,1)S(1)}, bf16[1,16,128]{2,1,0:T(8,128)(2,1)}, u32[]{:S(2)}) copy-start(bf16[1,16,128]{2,1,0:T(8,128)(2,1)} %query.1) | copy-start | bytes 12292
  3.9 0.7 %copy-start.2 = (f32[16]{0:T(128)S(1)}, f32[16]{0:T(128)}, u32[]{:S(2)}) copy-start(f32[16]{0:T(128)} %param.12) | copy-start | bytes 196
  4.6 0.7 %copy-start.3 = (f32[16]{0:T(128)S(1)}, f32[16]{0:T(128)}, u32[]{:S(2)}) copy-start(f32[16]{0:T(128)} %decay.1) | copy-start | bytes 196
  5.2 0.7 %copy-start.4 = (f32[128]{0:T(128)S(1)}, f32[128]{0:T(128)}, u32[]{:S(2)}) copy-start(f32[128]{0:T(128)} %param.15) | copy-start | bytes 1540

commit v2 on v1

v2 whole, which is shorter than its diff:
```python
import functools

import jax
import jax.numpy as jnp
from jax import lax
from jax.experimental import pallas as pl
from jax.experimental.pallas import tpu as pltpu
from jax.sharding import PartitionSpec as P

MESH = pl.DeviceIdType.MESH
F32 = jnp.float32
BF16 = jnp.bfloat16


def dot(left, right, contract=((1,), (0,))):
    return lax.dot_general(left, right, (contract, ((), ())), preferred_element_type=F32)


def level_masks(size):
    row = lax.broadcasted_iota(jnp.int32, (size, size), 0)
    col = lax.broadcasted_iota(jnp.int32, (size, size), 1)
    masks = []
    for level in range((size - 1).bit_length()):
        together = (row >> (level + 1)) == (col >> (level + 1))
        apart = (row >> level) != (col >> level)
        masks.append((together & apart & (row > col)).astype(F32).astype(BF16))
    return masks


def span(heads, masks, eye):
    keys_t, rights, grams, inverses = [], [], [], []
    for key, value, strength, fade in heads:
        key = key.astype(F32)
        key = key * lax.rsqrt(jnp.sum(key * key, axis=1, keepdims=True) + 1.0)
        weighted = (key * strength).astype(BF16)
        key = key.astype(BF16)
        value = (value.astype(F32) * (strength * fade)).astype(BF16)
        keys_t.append(key)
        rights.append(jnp.concatenate([value, weighted], axis=1))
        grams.append(dot(weighted, key, ((1,), (1,))).astype(BF16))
    for gram in grams:
        inverses.append(eye[...] - gram * masks[0])
    size = grams[0].shape[0]
    levels = (size - 1).bit_length()
    for level in range(1, levels - 1):
        steps = [dot(g * masks[level], x).astype(BF16) for g, x in zip(grams, inverses)]
        inverses = [x - dot(x, s).astype(BF16) for x, s in zip(inverses, steps)]
    half = size // 2
    out = []
    for key, right, gram, x in zip(keys_t, rights, grams, inverses):
        first, last = x[:half, :half], x[half:, half:]
        cross = dot(last, dot(gram[half:, :half], first).astype(BF16)).astype(BF16)
        top, low = key[:half], key[half:]
        y_first = dot(top, first, ((0,), (0,))) - dot(low, cross, ((0,), (0,)))
        y_last = dot(low, last, ((0,), (0,)))
        y = jnp.concatenate([y_first.astype(BF16), y_last.astype(BF16)], axis=1)
        out.append(dot(y, right))
    return out


def kernel(
    n, tp, groups, per, dim, together,
    prompt, key_w, value_w, beta_w, bias, decay, query, gain,
    state_out, read_out,
    feat, first_buf, rest_buf, total, beta_buf, bias_buf, decay_buf, query_buf, gain_buf,
    mask_buf, eye_buf, strength_buf, spans, partner_spans, joined, recv,
    row_stage, row_recv, read_stage, read_recv,
    in_sem, feat_send, feat_recv, first_sem, rest_sem, pair_send, pair_recv,
    map_send, map_recv, row_send, row_got, read_send, read_got,
):
    me = lax.axis_index("sp")
    core = lax.axis_index("tp")
    seg, part = prompt.shape[1], prompt.shape[2]
    wide = per * dim
    full = seg * n
    stride = n // groups
    half = groups // 2
    parity = lax.rem(me, 2)
    mine = me // stride
    slots = first_buf.shape[0]

    def owner(g):
        return g * stride + (lax.rem(g, 2) if stride > 1 else 0)

    is_owner = me == owner(mine)

    def when_owner(work):
        if stride == 1:
            work()
        else:
            pl.when(is_owner)(work)

    def pair_at(j):
        return lax.rem(mine // 2 + 1 + j, half)

    def group_at(index):
        keep = index // half
        return 2 * pair_at(lax.rem(index, half)) + keep * parity + (1 - keep) * (1 - parity)

    def columns(g):
        return pl.ds(pl.multiple_of(g * wide, wide), wide)

    def features_of(d):
        return pl.ds(pl.multiple_of(lax.rem(core + d, tp) * part, part), part)

    def fetch_first(index):
        slot = lax.rem(index, slots)
        return [
            pltpu.make_async_copy(
                w.at[features_of(0), columns(group_at(index))], first_buf.at[slot, j], first_sem.at[slot, j]
            )
            for j, w in enumerate((key_w, value_w))
        ]

    def fetch_rest(step):
        slot = lax.rem(step, 2)
        return [
            pltpu.make_async_copy(
                w.at[features_of(d), columns(group_at(step * together + s))],
                rest_buf.at[slot, s, j, d - 1], rest_sem.at[slot, s, j, d - 1],
            )
            for s in range(together)
            for j, w in enumerate((key_w, value_w))
            for d in range(1, tp)
        ]

    own_prompt = pltpu.make_async_copy(prompt.at[0], feat.at[core], in_sem.at[0])
    small = [
        pltpu.make_async_copy(src, dst, in_sem.at[1 + k])
        for k, (src, dst) in enumerate(
            ((beta_w, beta_buf), (bias, bias_buf), (decay, decay_buf), (query, query_buf), (gain, gain_buf))
        )
    ]
    own_prompt.start()
    for index in range(min(slots - 1, groups)):
        for copy in fetch_first(index):
            copy.start()
    for copy in small:
        copy.start()

    barrier = pltpu.get_barrier_semaphore()
    for d in range(1, n):
        pl.semaphore_signal(barrier, inc=1, device_id={"sp": lax.rem(me + d, n)}, device_id_type=MESH)
    for d in range(1, tp):
        pl.semaphore_signal(barrier, inc=1, device_id={"tp": lax.rem(core + d, tp)}, device_id_type=MESH)
    own_prompt.wait()
    pl.semaphore_wait(barrier, n - 1 + tp - 1)

    def feature_copy(d, slot):
        return pltpu.make_async_remote_copy(
            src_ref=feat.at[core], dst_ref=feat.at[slot],
            send_sem=feat_send.at[d - 1], recv_sem=feat_recv.at[slot],
            device_id={"tp": lax.rem(core + d, tp)}, device_id_type=MESH,
        )

    for d in range(1, tp):
        feature_copy(d, core).start()

    def project_first(index, carry):
        @pl.when(index + slots - 1 < groups)
        def _():
            for copy in fetch_first(index + slots - 1):
                copy.start()

        for copy in fetch_first(index):
            copy.wait()
        slot, g = lax.rem(index, slots), group_at(index)
        for j in range(2):
            total[g, j] = dot(feat[core], first_buf[slot, j])
        return carry

    lax.fori_loop(0, groups, project_first, 0)
    for copy in fetch_rest(0):
        copy.start()

    for level, mask in enumerate(level_masks(seg)):
        mask_buf[level] = mask
    ids = [lax.broadcasted_iota(jnp.int32, (seg, seg), axis) for axis in (0, 1)]
    eye_buf[...] = (ids[0] == ids[1]).astype(F32).astype(BF16)
    for copy in small:
        copy.wait()
    before = dot(feat[core], beta_buf[:, features_of(0)], ((1,), (1,)))
    for d in range(1, tp):
        other = lax.rem(core + d, tp)
        feature_copy(d, other).wait_recv()
        before += dot(feat[other], beta_buf[:, features_of(d)], ((1,), (1,)))
    strength_buf[...] = jax.nn.sigmoid(before + bias_buf[...])

    def pair_copy(m):
        return pltpu.make_async_remote_copy(
            src_ref=spans.at[0, m], dst_ref=partner_spans.at[m],
            send_sem=pair_send.at[m], recv_sem=pair_recv.at[m],
            device_id={"sp": me + 1 - 2 * parity}, device_id_type=MESH,
        )

    def map_copy(m, slot):
        return pltpu.make_async_remote_copy(
            src_ref=joined.at[m], dst_ref=recv.at[slot],
            send_sem=map_send.at[m], recv_sem=map_recv.at[slot],
            device_id={"sp": owner(2 * m + parity)}, device_id_type=MESH,
        )

    def send(step):
        for s in range(together):
            index = step * together + s
            m = pair_at(lax.rem(index, half))

            @pl.when(index < half)
            def _():
                pair_copy(m).start()

            @pl.when((index >= half) & (owner(2 * m + parity) != me))
            def _():
                map_copy(m, me // 2).start()

    def body(step, carry):
        slot = lax.rem(step, 2)

        @pl.when(step + 1 < groups // together)
        def _():
            for copy in fetch_rest(step + 1):
                copy.start()

        for copy in fetch_rest(step):
            copy.wait()
        projected = []
        for s in range(together):
            g = group_at(step * together + s)
            pair = []
            for j in range(2):
                acc = total[g, j]
                for d in range(1, tp):
                    acc += dot(feat[lax.rem(core + d, tp)], rest_buf[slot, s, j, d - 1])
                pair.append(acc.astype(BF16))
            projected.append(pair)

        @pl.when(step > 0)
        def _():
            send(step - 1)

        strengths = strength_buf[...]
        rates = decay_buf[...]
        lane = lax.broadcasted_iota(jnp.int32, strengths.shape, 1)
        rest = full - 1 - me * seg - lax.broadcasted_iota(jnp.int32, (seg, 1), 0)
        rest = rest.astype(F32) * (1.0 / full)
        heads = []
        for s in range(together):
            g = group_at(step * together + s)
            keys, values = projected[s]
            for h in range(per):
                head = g * per + h
                strength = jnp.sum(jnp.where(lane == head, strengths, 0.0), axis=1, keepdims=True)
                rate = jnp.sum(jnp.where(lane[:1] == head, rates, 0.0), axis=1, keepdims=True)
                fade = jnp.exp(-rate * rest)
                cols = slice(h * dim, (h + 1) * dim)
                heads.append((keys[:, cols], values[:, cols], strength, fade))
        keep = step * together // half
        for k, result in enumerate(span(heads, mask_buf, eye_buf)):
            m = pair_at(lax.rem(step * together + k // per, half))
            spans[keep, m, k % per] = result.astype(BF16)

        @pl.when(keep == 1)
        def _():
            for s in range(together):
                m = pair_at(lax.rem(step * together + s, half))
                pair_copy(m).wait_recv()
                for h in range(per):
                    ours, theirs = spans[1, m, h], partner_spans[m, h]
                    early = jnp.where(parity == 1, theirs, ours)
                    late = jnp.where(parity == 1, ours, theirs)
                    both = early.astype(F32) + late.astype(F32) - dot(late[:, dim:], early)
                    joined[m, h] = both.astype(BF16)

        return carry

    lax.fori_loop(0, groups // together, body, 0)
    recv[me // 2] = joined[mine // 2]
    send(groups // together - 1)

    rows = dim // n

    def row_copy(q, slot):
        return pltpu.make_async_remote_copy(
            src_ref=row_stage.at[q], dst_ref=row_recv.at[slot],
            send_sem=row_send.at[q], recv_sem=row_got.at[slot],
            device_id={"sp": q}, device_id_type=MESH,
        )

    def read_copy(q, slot):
        return pltpu.make_async_remote_copy(
            src_ref=read_stage, dst_ref=read_recv.at[slot],
            send_sem=read_send.at[q], recv_sem=read_got.at[slot],
            device_id={"sp": q}, device_id_type=MESH,
        )

    def finish():
        def link(p, states):
            @pl.when(p != me // 2)
            def _():
                map_copy(0, p).wait_recv()

            new = []
            for h in range(per):
                write, drop = recv[p, h, :, :dim].astype(F32), recv[p, h, :, dim:]
                high = states[h].astype(BF16)
                low = (states[h] - high.astype(F32)).astype(BF16)
                new.append(states[h] + (write - dot(drop, high) - dot(drop, low)))
            return tuple(new)

        states = lax.fori_loop(0, n // 2, link, tuple(jnp.zeros((dim, dim), F32) for _ in range(per)))
        for h in range(per):
            cast = states[h].astype(BF16)
            for q in range(n):
                row_stage[q, h] = cast[q * rows:(q + 1) * rows]
        unit = query_buf[0].astype(F32)
        unit = unit * lax.rsqrt(jnp.sum(unit * unit, axis=1, keepdims=True) + 1.0)
        which = lax.broadcasted_iota(jnp.int32, unit.shape, 0)
        for h in range(per):
            row = jnp.sum(jnp.where(which == mine * per + h, unit, 0.0), axis=0, keepdims=True)
            raw = jnp.dot(
                jnp.broadcast_to(row, (8, dim)), states[h],
                precision=lax.Precision.HIGHEST, preferred_element_type=F32,
            )[0:1]
            raw = raw * lax.rsqrt(jnp.mean(raw * raw, axis=1, keepdims=True) + 0.05) * gain_buf[...]
            read_stage[h:h + 1] = raw
        for d in range(1, n):
            row_copy(lax.rem(me + d, n), mine).start()
        for d in range(1, n):
            read_copy(lax.rem(me + d, n), mine).start()
        row_recv[mine] = row_stage[me]
        read_recv[mine] = read_stage[...]

    when_owner(finish)

    for g in range(groups):
        @pl.when(me != owner(g))
        def _():
            row_copy(me, g).wait_recv()
            read_copy(me, g).wait_recv()

        for h in range(per):
            state_out[0, g * per + h] = row_recv[g, h]
        read_out[0, g * per:(g + 1) * per] = read_recv[g]

    for d in range(1, tp):
        feature_copy(d, core).wait_send()
    for m in range(half):
        pair_copy(m).wait_send()

        @pl.when(owner(2 * m + parity) != me)
        def _():
            map_copy(m, 0).wait_send()

    def sent():
        for d in range(1, n):
            row_copy(lax.rem(me + d, n), mine).wait_send()
            read_copy(lax.rem(me + d, n), mine).wait_send()

    when_owner(sent)


def solution(mesh):
    n, tp = mesh.shape["sp"], mesh.shape["tp"]

    def shards(prompt, key_w, value_w, beta_w, bias, decay, query, gain):
        seg, part = prompt.shape[1:]
        depth = key_w.shape[0]
        heads = beta_w.shape[1]
        dim = key_w.shape[1] // heads
        per = max(1, heads // n)
        groups = heads // per
        wide = per * dim
        rows = dim // n
        levels = (seg - 1).bit_length()
        dma = pltpu.SemaphoreType.DMA
        vmem = pl.BlockSpec(memory_space=pltpu.VMEM)
        hbm = pl.BlockSpec(memory_space=pl.ANY)
        half = groups // 2
        together = min(2, half)
        slots = 4
        return pl.pallas_call(
            functools.partial(kernel, n, tp, groups, per, dim, together),
            out_shape=(
                jax.ShapeDtypeStruct((1, heads, rows, dim), BF16),
                jax.ShapeDtypeStruct((1, heads, dim), F32),
            ),
            in_specs=[hbm] * 8,
            out_specs=(vmem, vmem),
            scratch_shapes=[
                pltpu.VMEM((tp, seg, part), BF16),
                pltpu.VMEM((slots, 2, part, wide), BF16),
                pltpu.VMEM((2, together, 2, tp - 1, part, wide), BF16),
                pltpu.VMEM((groups, 2, seg, wide), F32),
                pltpu.VMEM((heads, depth), BF16),
                pltpu.VMEM((1, heads), F32),
                pltpu.VMEM((1, heads), F32),
                pltpu.VMEM((1, heads, dim), BF16),
                pltpu.VMEM((1, dim), F32),
                pltpu.VMEM((levels, seg, seg), BF16),
                pltpu.VMEM((seg, seg), BF16),
                pltpu.VMEM((seg, heads), F32),
                pltpu.VMEM((2, half, per, dim, 2 * dim), BF16),
                pltpu.VMEM((half, per, dim, 2 * dim), BF16),
                pltpu.VMEM((half, per, dim, 2 * dim), BF16),
                pltpu.VMEM((n // 2, per, dim, 2 * dim), BF16),
                pltpu.VMEM((n, per, rows, dim), BF16),
                pltpu.VMEM((groups, per, rows, dim), BF16),
                pltpu.VMEM((per, dim), F32),
                pltpu.VMEM((groups, per, dim), F32),
                dma((6,)),
                dma((tp - 1,)),
                dma((tp,)),
                dma((slots, 2)),
                dma((2, together, 2, tp - 1)),
                dma((half,)),
                dma((half,)),
                dma((half,)),
                dma((n // 2,)),
                dma((n,)),
                dma((groups,)),
                dma((n,)),
                dma((groups,)),
            ],
            compiler_params=pltpu.CompilerParams(
                collective_id=0, has_side_effects=True, vmem_limit_bytes=60 * 2**20
            ),
        )(
            prompt, key_w, value_w, beta_w.T, bias.reshape(1, heads), decay.reshape(1, heads),
            query, gain.reshape(1, dim),
        )

    return jax.shard_map(
        shards,
        mesh=mesh,
        in_specs=(
            P("gr", "sp", "tp"),
            P(None, "tp"),
            P(None, "tp"),
            P(None, "tp"),
            P("tp"),
            P("tp"),
            P("gr", "tp", None),
            P(),
        ),
        out_specs=(P("gr", "tp", "sp", None), P("gr", "tp", None)),
        check_vma=False,
    )
```

time: 61.6 us -> 54 us (0.88)
  Pallas kernels: 54.3 us -> 50.4 us
  local copies, waits for them, and re-layouts: 6.48 us -> 2.77 us
    pallas_call x1, Pallas kernels: 54.3 us -> 50.4 us  [shards(): pl.pallas_call(functools.partial(kernel, n, tp, groups, per, dim, togethe...]
    unnamed x13 -> x2, local copies, waits for them, and re-layouts: 6.48 us -> 2.77 us
where the time goes in v2:
time: 54 us; the launch traced here: 53.8 us
  Pallas kernels  50.4 us (93%)
  local copies, waits for them, and re-layouts  2.77 us (5%)
  between operations  0.64 us (1%)
    pallas_call x1, Pallas kernels, shards(): pl.pallas_call(functools.partial(kernel, n, tp, groups, per, dim, togethe...  50.4 us
    unnamed x2, local copies, waits for them, and re-layouts  2.77 us

profile of v2, /device:TPU:0, one launch (start us, length us, event | category | flops | bytes accessed | tf_op | source)
XLA Modules:
  0.0 53.8 jit_solution(8982925185550376833)
XLA Ops:
  0.6 50.4 %shard_map.95 = (bf16[1,16,16,128]{3,2,1,0:T(8,128)(2,1)}, f32[1,16,128]{2,1,0:T(8,128)}) custom-call(bf16[1,256,2048]{2,1,0:T(8,128)(2,1)} %prompt.1, bf16[4096,2048]{1,0:T(8,128)(2,1)} %key_w.1, bf16[4096,2048]{1,0:T(8,128)(2,1)} %value_w.1, bf16[16,4096]{1,0:T(8,128)(2,1)} %bitcast.4, f32[1,16]{1,0:T(1,128)} %bitcast.5, f32[1,16]{1,0:T(1,128)} %bitcast.6, ...), custom_call_target="tpu_custom_call" | custom-call | tf_op jit(solution)/shard_map/pallas_call | solution.py:381
  51.0 1.5 %copy.12 = bf16[1,16,16,128]{3,2,1,0:T(8,128)(2,1)} copy(bf16[1,16,16,128]{3,2,1,0:T(8,128)(2,1)} %get-tuple-element.4) | data formatting | bytes 131072
  52.5 1.3 %copy.13 = f32[1,16,128]{2,1,0:T(8,128)} copy(f32[1,16,128]{2,1,0:T(8,128)} %get-tuple-element.5) | data formatting | bytes 16384
